TPU v7x, 32 devices: a whole 2x2x4 slice. The times are simulated.
32 devices in a mesh: ep: 16 (over z, y, core), tp: 2 (over x).
Axes of the slice: x: 2, y: 2, z: 4, core: 2. Of those that a mesh axis runs over, the one named last changes fastest.
Arguments:
- tokens: bfloat16 [128, 2048], P('ep'), may hold values from -48 to 48
- past_lengths: int32 [128], P('ep'), may hold values from 1024 to 16383
- state: float32 [128, 16, 128, 256], P('ep', 'tp'), may hold values from -0.625 to 0.625
- norm1_gain: float32 [2048], replicated, may hold values from 0.1 to 1.9
- query_weight: bfloat16 [2048, 2048], P(None, 'tp'), may hold values from -0.125 to 0.125
- key_weight: bfloat16 [2048, 2048], P(None, 'tp'), may hold values from -0.125 to 0.125
- value_weight: bfloat16 [2048, 4096], P(None, 'tp'), may hold values from -0.125 to 0.125
- out_weight: bfloat16 [4096, 2048], P('tp'), may hold values from -0.09375 to 0.09375
- norm2_gain: float32 [2048], replicated, may hold values from 0.1 to 1.9
- branch_gate: float32 [2048], replicated, may hold values from -0.125 to 0.125
- route_ids: int32 [128, 2], P('ep'), may hold values from 0 to 3, all different within a row; in each aligned block of 8 rows (0 to 7, 8 to 15, ...) at most 8 rows name the same one
- route_weights: float32 [128, 2], P('ep'), may hold values from 0.2 to 1
- expert_gate: bfloat16 [16, 2048, 1792], P('ep', None, 'tp'), may hold values from -0.125 to 0.125
- expert_up: bfloat16 [16, 2048, 1792], P('ep', None, 'tp'), may hold values from -0.125 to 0.125
- expert_down: bfloat16 [16, 1792, 2048], P('ep', 'tp'), may hold values from -0.0625 to 0.0625
- dense_gate: bfloat16 [2048, 5632], P('tp', 'ep'), may hold values from -0.125 to 0.125
- dense_up: bfloat16 [2048, 5632], P('tp', 'ep'), may hold values from -0.125 to 0.125
- dense_down: bfloat16 [5632, 2048], P('ep', 'tp'), may hold values from -0.15625 to 0.15625
Outputs:
- layer_out: bfloat16 [128, 2048], P('ep', 'tp')
- new_state: float32 [128, 16, 128, 256], P('ep', 'tp')
Inputs may be any that keep to these rules, and one draw needn't show every extreme that they name: `route_ids`: in each aligned block of 8 rows no expert is named by more than 8 rows, and some block names one expert exactly 8 times.
All inputs are finite; a program needn't handle non-finite values.
Results may differ from a plain program's by a relative error of at most 0.006.
Values may be sent and summed in bfloat16 or wider, within the bound.
A program may use at most 128 MiB of HBM per device.

v0:
```python
import functools

import jax
import jax.numpy as jnp
from jax import lax
from jax.experimental import pallas as pl
from jax.experimental.pallas import tpu as pltpu
from jax.sharding import PartitionSpec as P

MESH = pl.DeviceIdType.MESH

RMS_EPSILON = 1e-06
GROUP_EPSILON = 1e-05


def head_decay(head_index, head_total):
    return jnp.exp(
        jnp.log1p(-jnp.exp2(-5.0 - 7.0 * head_index.astype(jnp.float32) / (head_total - 1)))
    )


def rotate_heads(features, positions):
    half_size = features.shape[-1] // 2
    inverse = 10000.0 ** (-jnp.arange(half_size, dtype=jnp.float32) / half_size)
    angles = positions.astype(jnp.float32)[:, None] * inverse[None, :]
    cosine = jnp.cos(angles)[:, None, :]
    sine_part = jnp.sin(angles)[:, None, :]
    first_half = features[..., :half_size]
    second_half = features[..., half_size:]
    return jnp.concatenate(
        [
            first_half * cosine - second_half * sine_part,
            first_half * sine_part + second_half * cosine,
        ],
        axis=-1,
    )


def retention_step(
    normed_in, positions, state, query_weight, key_weight, value_weight, head_index, head_total
):
    row_count, head_count, key_size, value_size = state.shape
    query = jnp.dot(normed_in, query_weight, preferred_element_type=jnp.float32).reshape(
        row_count, head_count, key_size
    )
    keys = jnp.dot(normed_in, key_weight, preferred_element_type=jnp.float32).reshape(
        row_count, head_count, key_size
    )
    values = jnp.dot(normed_in, value_weight, preferred_element_type=jnp.float32).reshape(
        row_count, head_count, value_size
    )
    query = rotate_heads(query, positions)
    keys = rotate_heads(keys, positions) * key_size ** (-0.5)
    decay = head_decay(head_index, head_total)
    new_state = state * decay[None, :, None, None] + keys[:, :, :, None] * values[:, :, None, :]
    retained = jnp.einsum("shk,shkv->shv", query, new_state)
    centered = retained - jnp.mean(retained, axis=-1, keepdims=True)
    normed = centered * lax.rsqrt(
        jnp.mean(centered * centered, axis=-1, keepdims=True) + GROUP_EPSILON
    )
    return (normed.astype(jnp.bfloat16).reshape(row_count, head_count * value_size), new_state)


LANES = 128
HALF = LANES // 2
LAST_DIMS = (((1,), (1,)), ((), ()))


def await_bytes(ref, semaphore):
    pltpu.make_async_copy(ref, ref, semaphore).wait()


def tail_kernel(
    ep_count,
    tp_count,
    partial_ref,
    token_ref,
    gain_ref,
    gate_ref,
    route_ref,
    expert_gate,
    expert_up,
    expert_down,
    dense_gate,
    dense_up,
    dense_down,
    out_ref,
    pair_w,
    down_w,
    dense_gate_w,
    dense_up_w,
    dense_down_w,
    partials,
    mixed_ref,
    message,
    gathered,
    normed_ref,
    dense_part,
    dense_parts,
    hidden_ref,
    outgoing,
    arrived,
    sems,
):
    ep = lax.axis_index("ep")
    tp = lax.axis_index("tp")
    device_count = ep_count * tp_count
    here = ep * tp_count + tp
    rows, width = partial_ref.shape
    token_count = ep_count * rows
    col_width = width // tp_count
    tiles = pair_w.shape[0]

    def copy_tile(j):
        cols = pl.ds(j * LANES, LANES)
        pltpu.make_async_copy(
            expert_gate.at[0, :, cols], pair_w.at[j, :, pl.ds(0, LANES)], sems.at[0]
        ).start()
        pltpu.make_async_copy(
            expert_up.at[0, :, cols], pair_w.at[j, :, pl.ds(LANES, LANES)], sems.at[0]
        ).start()

    pltpu.make_async_copy(dense_gate, dense_gate_w, sems.at[2]).start()
    pltpu.make_async_copy(dense_up, dense_up_w, sems.at[3]).start()
    for j in range(tiles):
        copy_tile(j)
    pltpu.make_async_copy(expert_down.at[0], down_w, sems.at[1]).start()
    pltpu.make_async_copy(dense_down, dense_down_w, sems.at[4]).start()

    barrier = pltpu.get_barrier_semaphore()

    def greet(k, carry):
        other = lax.rem(here + k, device_count)
        pl.semaphore_signal(
            barrier,
            inc=1,
            device_id=(lax.div(other, tp_count), lax.rem(other, tp_count)),
            device_id_type=MESH,
        )
        return carry

    lax.fori_loop(1, device_count, greet, 0)
    pl.semaphore_wait(barrier, device_count - 1)

    def to_tp(source, target, send, receive):
        pltpu.make_async_copy(source, target.at[tp], receive).start()

        def one(k, carry):
            pltpu.make_async_remote_copy(
                src_ref=source,
                dst_ref=target.at[tp],
                send_sem=send,
                recv_sem=receive,
                device_id=(ep, lax.rem(tp + k, tp_count)),
                device_id_type=MESH,
            ).start()
            return carry

        lax.fori_loop(1, tp_count, one, 0)

    to_tp(partial_ref, partials, sems.at[5], sems.at[6])
    await_bytes(partials, sems.at[6])
    mixed = token_ref[...].astype(jnp.float32) + jnp.sum(partials[...], axis=0)
    mixed_ref[...] = mixed
    scale = lax.rsqrt(jnp.mean(mixed * mixed, axis=-1, keepdims=True) + RMS_EPSILON)
    scaled = mixed * scale * gain_ref[...]
    along = jnp.sum(scaled * gate_ref[...], axis=-1, keepdims=True)
    branch_weight = 1.0 / (1.0 + jnp.exp(-along))
    lane = lax.broadcasted_iota(jnp.int32, (rows, LANES), 1)
    factors = jnp.where(lane == HALF - 1, branch_weight, route_ref[...])
    high = factors.astype(jnp.bfloat16).astype(jnp.float32)
    low = pltpu.roll(factors - high, HALF, 1)
    message[0, :, pl.ds(0, width)] = scaled.astype(jnp.bfloat16)
    message[0, :, pl.ds(width, LANES)] = jnp.where(lane < HALF, high, low).astype(jnp.bfloat16)

    pltpu.make_async_copy(message.at[0], gathered.at[ep], sems.at[8]).start()

    def spread(k, carry):
        pltpu.make_async_remote_copy(
            src_ref=message.at[0],
            dst_ref=gathered.at[ep],
            send_sem=sems.at[7],
            recv_sem=sems.at[8],
            device_id=(lax.rem(ep + k, ep_count), tp),
            device_id_type=MESH,
        ).start()
        return carry

    lax.fori_loop(1, ep_count, spread, 0)
    await_bytes(gathered, sems.at[8])
    normed_ref[...] = (
        gathered[:, :, pl.ds(0, width)]
        .astype(jnp.float32)
        .reshape(token_count, width)
        .astype(jnp.bfloat16)
    )
    tail_lanes = (
        gathered[:, :, pl.ds(width, LANES)].astype(jnp.float32).reshape(token_count, LANES)
    )
    place = lax.rem(lax.broadcasted_iota(jnp.int32, (token_count, LANES), 1), HALF)
    expert = lax.div(ep, 4)
    expert_factor = jnp.sum(jnp.where(place == expert, tail_lanes, 0.0), axis=1, keepdims=True)
    branch_factor = jnp.sum(jnp.where(place == HALF - 1, tail_lanes, 0.0), axis=1, keepdims=True)

    features = dense_gate_w.shape[1]
    own_features = pl.ds(pl.multiple_of(tp * features, LANES), features)
    await_bytes(dense_gate_w, sems.at[2])
    await_bytes(dense_up_w, sems.at[3])
    feature_values = normed_ref[:, own_features]
    dense_part[0] = lax.dot_general(
        feature_values, dense_gate_w[...], LAST_DIMS, preferred_element_type=jnp.float32
    ).astype(jnp.bfloat16)
    dense_part[1] = lax.dot_general(
        feature_values, dense_up_w[...], LAST_DIMS, preferred_element_type=jnp.float32
    ).astype(jnp.bfloat16)
    to_tp(dense_part, dense_parts, sems.at[9], sems.at[10])

    await_bytes(pair_w, sems.at[0])

    def expert_tile(j, carry):
        both = jnp.dot(normed_ref[...], pair_w[j], preferred_element_type=jnp.float32)
        gate_value, up_value = both[:, :LANES], both[:, LANES:]
        hidden_ref[:, pl.ds(pl.multiple_of(j * LANES, LANES), LANES)] = (
            gate_value / (1.0 + jnp.exp(-gate_value)) * up_value
        ).astype(jnp.bfloat16)
        return carry

    lax.fori_loop(0, tiles, expert_tile, 0)
    await_bytes(down_w, sems.at[1])
    step = min(2 * LANES, col_width)

    def expert_cols(part, t):
        cols = pl.ds(pl.multiple_of(part * col_width + t * step, LANES), step)
        return expert_factor * jnp.dot(
            hidden_ref[...], down_w[:, cols], preferred_element_type=jnp.float32
        )

    def put(part, t, value):
        outgoing[part, :, :, pl.ds(pl.multiple_of(t * step, LANES), step)] = value.reshape(
            ep_count, rows, step
        ).astype(jnp.bfloat16)

    def send_out(part, first):
        def one(k, carry):
            to = lax.rem(ep + k, ep_count)
            pltpu.make_async_remote_copy(
                src_ref=outgoing.at[part, to],
                dst_ref=arrived.at[here],
                send_sem=sems.at[11],
                recv_sem=sems.at[12],
                device_id=(to, part),
                device_id_type=MESH,
            ).start()
            return carry

        lax.fori_loop(first, ep_count + first - (1 if first else 0), one, 0)

    def other_part(k, carry):
        part = lax.rem(tp + k, tp_count)

        def tile(t, inner):
            put(part, t, expert_cols(part, t))
            return inner

        lax.fori_loop(0, col_width // step, tile, 0)
        send_out(part, 0)
        return carry

    lax.fori_loop(1, tp_count, other_part, 0)

    await_bytes(dense_parts, sems.at[10])
    await_bytes(dense_down_w, sems.at[4])
    whole = jnp.sum(dense_parts[...].astype(jnp.float32), axis=0)
    dense_hidden = (whole[0] / (1.0 + jnp.exp(-whole[0])) * whole[1]).astype(jnp.bfloat16)

    def own_tile(t, carry):
        cols = pl.ds(pl.multiple_of(t * step, LANES), step)
        dense = jnp.dot(dense_hidden, dense_down_w[:, cols], preferred_element_type=jnp.float32)
        put(tp, t, expert_cols(tp, t) + branch_factor * dense)
        return carry

    lax.fori_loop(0, col_width // step, own_tile, 0)
    pltpu.make_async_copy(outgoing.at[tp, ep], arrived.at[here], sems.at[12]).start()
    send_out(tp, 1)
    await_bytes(arrived, sems.at[12])

    def gather_sum(i, total):
        return total + jnp.sum(arrived[pl.ds(i * 8, 8)].astype(jnp.float32), axis=0)

    own_cols = pl.ds(pl.multiple_of(tp * col_width, LANES), col_width)
    out_ref[...] = lax.fori_loop(
        0, device_count // 8, gather_sum, mixed_ref[:, own_cols]
    ).astype(out_ref.dtype)
    await_bytes(partials.at[pl.ds(0, tp_count - 1)], sems.at[5])
    await_bytes(gathered.at[pl.ds(0, ep_count - 1)], sems.at[7])
    await_bytes(dense_parts.at[pl.ds(0, tp_count - 1)], sems.at[9])
    await_bytes(arrived.at[pl.ds(0, device_count - 1)], sems.at[11])


def tail(*operands):
    *arrays, ep_count, tp_count = operands
    partial, tokens = arrays[0], arrays[1]
    expert_gate, expert_down, dense_gate, dense_down = arrays[5], arrays[7], arrays[8], arrays[10]
    rows, width = partial.shape
    token_count = ep_count * rows
    col_width = width // tp_count
    expert_hidden = expert_gate.shape[2]
    dense_hidden = dense_gate.shape[0]
    bf16, f32 = jnp.bfloat16, jnp.float32
    vmem = pl.BlockSpec(memory_space=pltpu.VMEM)
    in_hbm = pl.BlockSpec(memory_space=pltpu.HBM)
    return pl.pallas_call(
        functools.partial(tail_kernel, ep_count, tp_count),
        out_shape=jax.ShapeDtypeStruct((rows, col_width), bf16),
        in_specs=[vmem] * 5 + [in_hbm] * 6,
        out_specs=vmem,
        scratch_shapes=[
            pltpu.VMEM((expert_hidden // LANES, width, 2 * LANES), bf16),
            pltpu.VMEM(expert_down.shape[1:], bf16),
            pltpu.VMEM(dense_gate.shape, bf16),
            pltpu.VMEM(dense_gate.shape, bf16),
            pltpu.VMEM(dense_down.shape, bf16),
            pltpu.VMEM((tp_count, rows, width), f32),
            pltpu.VMEM((rows, width), f32),
            pltpu.VMEM((1, rows, width + LANES), bf16),
            pltpu.VMEM((ep_count, rows, width + LANES), bf16),
            pltpu.VMEM((token_count, width), bf16),
            pltpu.VMEM((2, token_count, dense_hidden), bf16),
            pltpu.VMEM((tp_count, 2, token_count, dense_hidden), bf16),
            pltpu.VMEM((token_count, expert_hidden), bf16),
            pltpu.VMEM((tp_count, ep_count, rows, col_width), bf16),
            pltpu.VMEM((ep_count * tp_count, rows, col_width), bf16),
            pltpu.SemaphoreType.DMA((13,)),
        ],
        compiler_params=pltpu.CompilerParams(
            collective_id=0, has_side_effects=True, vmem_limit_bytes=62 * 1024 * 1024
        ),
    )(*arrays)


def local(
    tokens,
    past_lengths,
    state,
    norm1_gain,
    query_weight,
    key_weight,
    value_weight,
    out_weight,
    norm2_gain,
    branch_gate,
    route_ids,
    route_weights,
    expert_gate,
    expert_up,
    expert_down,
    dense_gate,
    dense_up,
    dense_down,
):
    tp_count = lax.axis_size("tp")
    ep_count = lax.axis_size("ep")
    heads_here = state.shape[1]
    head_index = lax.axis_index("tp") * heads_here + jnp.arange(heads_here)
    inputs = tokens.astype(jnp.float32)
    normed_in = (
        inputs
        * lax.rsqrt(jnp.mean(inputs * inputs, axis=-1, keepdims=True) + RMS_EPSILON)
        * norm1_gain
    ).astype(jnp.bfloat16)
    normed, new_state = retention_step(
        normed_in,
        past_lengths,
        state,
        query_weight,
        key_weight,
        value_weight,
        head_index,
        heads_here * tp_count,
    )
    partial_mix = jnp.dot(normed, out_weight, preferred_element_type=jnp.float32)
    lanes = jnp.arange(LANES, dtype=jnp.int32)
    named = (route_ids[:, :, None] == lanes[None, None, :]).astype(jnp.float32)
    route_lanes = jnp.sum(named * route_weights[:, :, None], axis=1)
    hidden_pad = -expert_gate.shape[2] % LANES
    if hidden_pad:
        expert_gate = jnp.pad(expert_gate, ((0, 0), (0, 0), (0, hidden_pad)))
        expert_up = jnp.pad(expert_up, ((0, 0), (0, 0), (0, hidden_pad)))
        expert_down = jnp.pad(expert_down, ((0, 0), (0, hidden_pad), (0, 0)))
    layer_out = tail(
        partial_mix,
        tokens,
        norm2_gain[None, :],
        branch_gate[None, :],
        route_lanes,
        expert_gate,
        expert_up,
        expert_down,
        dense_gate.T,
        dense_up.T,
        dense_down,
        ep_count,
        tp_count,
    )
    return (layer_out, new_state)


def solution(mesh):
    return jax.shard_map(
        local,
        mesh=mesh,
        in_specs=(
            P("ep", None),
            P("ep"),
            P("ep", "tp", None, None),
            P(),
            P(None, "tp"),
            P(None, "tp"),
            P(None, "tp"),
            P("tp", None),
            P(),
            P(),
            P("ep", None),
            P("ep", None),
            P("ep", None, "tp"),
            P("ep", None, "tp"),
            P("ep", "tp", None),
            P("tp", "ep"),
            P("tp", "ep"),
            P("ep", "tp"),
        ),
        out_specs=(P("ep", "tp"), P("ep", "tp", None, None)),
        check_vma=False,
    )
```

profile of v0, /device:TPU:0, one launch (start us, length us, event | category | flops | bytes accessed | tf_op | source)
XLA Modules:
  0.0 66.3 jit_solution(3356992267579514098)
XLA Ops:
  0.6 0.9 %fusion = f32[8]{0:T(128)S(1)} fusion(bf16[8,2048]{1,0:T(8,128)(2,1)} %token_ref.1), kind=kLoop, calls=%fused_computation.5 | loop fusion | flops 49144 | bytes 32800 | tf_op jit(solution)/shard_map/reduce_sum | solution.py:368
  1.5 2.9 %convolution_bitcast_fusion = f32[8,8,128]{2,0,1:T(8,128)S(1)} fusion(bf16[2048,1024]{1,0:T(8,128)(2,1)} %param.23, bf16[8,2048]{1,0:T(8,128)(2,1)} %token_ref.1, f32[2048]{0:T(1024)} %param.21, f32[8]{0:T(128)S(1)} %add_rsqrt_fusion.1), kind=kOutput, calls=%fused_computation.1 | convolution fusion | flops 33619968 | bytes 4268064 | tf_op jit(solution)/shard_map/dot_general | solution.py:46
  4.4 0.7 %convert_element_type.23 = f32[8]{0:T(128)S(1)} convert(s32[8]{0:T(128)} %param.19) | non-fusion elementwise | flops 8 | bytes 64 | tf_op jit(solution)/shard_map/convert_element_type | solution.py:25
  5.1 0.1 multiply_cosine_fusion
  5.2 0.1 multiply_subtract_fusion
  5.3 0.1 maximum_multiply_fusion
  5.4 4.6 %fusion.6 = f32[8,2048]{1,0:T(8,128)S(1)} fusion(bf16[2048,2048]{1,0:T(8,128)(2,1)} %param.24, bf16[8,2048]{1,0:T(8,128)(2,1)} %token_ref.1, f32[2048]{0:T(1024)} %param.21, f32[8]{0:T(128)S(1)} %add_rsqrt_fusion.1), kind=kOutput, calls=%fused_computation.30 | convolution fusion | flops 67174400 | bytes 8495136 | tf_op jit(solution)/shard_map/dot_general | solution.py:49
  10.1 0.0 slice-start
  10.1 0.0 copy-start.1
  10.1 0.0 copy-start.2
  10.2 0.0 copy-start.3
  10.2 0.0 slice-start.1
  10.2 4.3 %multiply_add_fusion = f32[8,8,128,256]{3,2,1,0:T(8,128)S(1)} fusion(f32[8,8,128,256]{3,2,1,0:T(8,128)} %param.20, f32[8,8,256]{2,1,0:T(8,128)S(1)} %copy.25, f32[8,8,128]{2,1,0:T(8,128)S(1)} %copy.24, f32[8]{0:T(128)S(1)} %log-plus-one_exponential_fusion), kind=kLoop, calls=%fused_computation | loop fusion | flops 6291456 | bytes 16875552 | tf_op jit(solution)/shard_map/add | solution.py:55
  14.5 0.5 copy-done.1
  14.9 0.0 copy-done.2
  14.9 0.0 copy-done.3
  14.9 0.0 copy-start
  14.9 0.7 %convolution_bitcast_fusion.1 = f32[8,8,128]{2,0,1:T(8,128)S(1)} fusion(bf16[2048,1024]{1,0:T(8,128)(2,1)S(1)} %copy-done.1, bf16[8,2048]{1,0:T(8,128)(2,1)S(1)} %copy-done.2, f32[2048]{0:T(1024)S(1)} %copy-done.3, f32[8]{0:T(128)S(1)} %add_rsqrt_fusion.1), kind=kOutput, calls=%fused_computation.2 | convolution fusion | flops 33619968 | bytes 4268064 | tf_op jit(solution)/shard_map/dot_general | solution.py:43
  15.6 0.1 multiply_subtract_fusion.1
  15.7 0.1 maximum_bitcast_fusion
  15.8 0.7 %fusion.4 = f32[8,8,1,256]{3,2,1,0:T(1,128)S(1)} fusion(f32[8,8,128,256]{3,2,1,0:T(8,128)S(1)} %multiply_add_fusion, bf16[8,8,128,1]{2,0,1,3:T(8,128)(2,1)S(1)} %maximum_bitcast_fusion), kind=kOutput, calls=%fused_computation.15 | convolution fusion | flops 4194304 | bytes 8470528 | tf_op jit(solution)/shard_map/shk,shkv->shv/dot_general | solution.py:56
  16.5 0.0 copy-start.4
  16.5 0.0 copy-start.5
  16.5 0.1 bitcast_reduce_fusion
  16.6 0.2 multiply_reduce_fusion
  16.7 0.1 fusion.3
  16.9 0.0 slice-done
  16.9 3.5 %slice-done.1 = s8[4194304]{0:T(1024)(128)(4,1)S(1)} async-done(((s8[8388608]{0:T(1024)(128)(4,1)}), s8[4194304]{0:T(1024)(128)(4,1)S(1)}, s32[]{:S(2)}) %slice-start.1) | async-done | bytes 4194328
  20.3 1.8 %fusion.10.partial_ref = f32[8,2048]{1,0:T(8,128)} fusion(bf16[8,2048]{1,0:T(8,128)(2,1)S(1)} %bitcast.33, bf16[2048,2048]{1,0:T(8,128)(2,1)S(1)} %bitcast.30), kind=kOutput, calls=%fused_computation.31 | convolution fusion | flops 67108864 | bytes 8486912 | tf_op jit(solution)/shard_map/dot_general | solution.py:381
  22.1 0.0 copy-done
  22.1 0.0 copy-done.4
  22.1 0.0 copy-done.5
  22.1 0.7 %select_reduce_fusion.route_ref = f32[8,128]{1,0:T(8,128)} fusion(f32[8,2]{0,1:T(2,128)S(1)} %copy-done.4, s32[8,2]{0,1:T(2,128)S(1)} %copy-done.5), kind=kLoop, calls=%fused_computation.21 | loop fusion | flops 5120 | bytes 4224 | tf_op jit(solution)/shard_map/reduce_sum | solution.py:384
  22.8 42.2 %shard_map.185 = bf16[8,1024]{1,0:T(8,128)(2,1)} custom-call(f32[8,2048]{1,0:T(8,128)} %fusion.10.partial_ref, bf16[8,2048]{1,0:T(8,128)(2,1)} %token_ref.1, f32[1,2048]{1,0:T(1,128)} %bitcast.35, f32[1,2048]{1,0:T(1,128)} %bitcast.36, f32[8,128]{1,0:T(8,128)} %select_reduce_fusion.route_ref, bf16[1,2048,896]{2,1,0:T(8,128)(2,1)} %expert_gate.1, ...), custom_call_target="tpu_custom_call" | custom-call | tf_op jit(solution)/shard_map/pallas_call | solution.py:312
  65.0 1.3 %copy.37 = bf16[8,1024]{1,0:T(8,128)(2,1)} copy(bf16[8,1024]{1,0:T(8,128)(2,1)} %shard_map.185) | data formatting | bytes 32768
  (9 shorter events, 0.1 us)
Async XLA Ops:
  10.1 6.8 %slice-start = ((s8[8388608]{0:T(1024)(128)(4,1)}), s8[4194304]{0:T(1024)(128)(4,1)S(1)}, s32[]{:S(2)}) async-start(s8[8388608]{0:T(1024)(128)(4,1)} %bitcast.29), calls=%async_computation | async-start | bytes 8388608
  10.1 4.8 %copy-start.1 = (bf16[2048,1024]{1,0:T(8,128)(2,1)S(1)}, bf16[2048,1024]{1,0:T(8,128)(2,1)}, u32[]{:S(2)}) copy-start(bf16[2048,1024]{1,0:T(8,128)(2,1)} %param.22) | copy-start | bytes 12582916
  10.1 4.8 %copy-start.2 = (bf16[8,2048]{1,0:T(8,128)(2,1)S(1)}, bf16[8,2048]{1,0:T(8,128)(2,1)}, u32[]{:S(2)}) copy-start(bf16[8,2048]{1,0:T(8,128)(2,1)} %token_ref.1) | copy-start | bytes 98308
  10.2 4.8 %copy-start.3 = (f32[2048]{0:T(1024)S(1)}, f32[2048]{0:T(1024)}, u32[]{:S(2)}) copy-start(f32[2048]{0:T(1024)} %param.21) | copy-start | bytes 24580
  10.2 10.2 %slice-start.1 = ((s8[8388608]{0:T(1024)(128)(4,1)}), s8[4194304]{0:T(1024)(128)(4,1)S(1)}, s32[]{:S(2)}) async-start(s8[8388608]{0:T(1024)(128)(4,1)} %bitcast.29), calls=%async_computation.1 | async-start | bytes 8388608
  14.9 7.2 %copy-start = (f32[8,8,128,256]{3,2,1,0:T(8,128)}, f32[8,8,128,256]{3,2,1,0:T(8,128)S(1)}, u32[]{:S(2)}) copy-start(f32[8,8,128,256]{3,2,1,0:T(8,128)S(1)} %multiply_add_fusion) | copy-start | bytes 25165828
  16.5 5.7 %copy-start.4 = (f32[8,2]{0,1:T(2,128)S(1)}, f32[8,2]{0,1:T(2,128)}, u32[]{:S(2)}) copy-start(f32[8,2]{0,1:T(2,128)} %param.29) | copy-start | bytes 196
  16.5 5.7 %copy-start.5 = (s32[8,2]{0,1:T(2,128)S(1)}, s32[8,2]{0,1:T(2,128)}, u32[]{:S(2)}) copy-start(s32[8,2]{0,1:T(2,128)} %param.28) | copy-start | bytes 196
where the time goes:
time: 66.6 us; the launch traced here: 66.3 us
  Pallas kernels  42.2 us (63%)
  matrix products  10.7 us (16%)
  other arithmetic  7.31 us (11%)
  local copies, waits for them, and re-layouts  5.35 us (8%)
  between operations  0.77 us (1%)
    pallas_call x1, Pallas kernels, tail(): pl.pallas_call(functools.partial(tail_kernel, ep_count, tp_count), out_sh...  42.2 us
    unnamed x18, local copies, waits for them, and re-layouts  5.31 us
    dot_general x1, matrix products, retention_step(): jnp.dot(normed_in, value_weight, preferred_element_type=jnp.float32)  4.64 us
    add x1, other arithmetic, retention_step(): state * decay[None, :, None, None]  4.27 us
    dot_general x1, matrix products, retention_step(): jnp.dot(normed_in, key_weight, preferred_element_type=jnp.float32)  2.91 us
    dot_general x1, matrix products, local(): jnp.dot(normed, out_weight, preferred_element_type=jnp.float32)  1.81 us

commit v1 on v0

v1 whole, which is shorter than its diff:
```python
import functools

import jax
import jax.numpy as jnp
from jax import lax
from jax.experimental import pallas as pl
from jax.experimental.pallas import tpu as pltpu
from jax.sharding import PartitionSpec as P

MESH = pl.DeviceIdType.MESH

RMS_EPSILON = 1e-06
GROUP_EPSILON = 1e-05


def head_decay(head_index, head_total):
    return jnp.exp(
        jnp.log1p(-jnp.exp2(-5.0 - 7.0 * head_index.astype(jnp.float32) / (head_total - 1)))
    )


def rotate_heads(features, positions):
    half_size = features.shape[-1] // 2
    inverse = 10000.0 ** (-jnp.arange(half_size, dtype=jnp.float32) / half_size)
    angles = positions.astype(jnp.float32)[:, None] * inverse[None, :]
    cosine = jnp.cos(angles)[:, None, :]
    sine_part = jnp.sin(angles)[:, None, :]
    first_half = features[..., :half_size]
    second_half = features[..., half_size:]
    return jnp.concatenate(
        [
            first_half * cosine - second_half * sine_part,
            first_half * sine_part + second_half * cosine,
        ],
        axis=-1,
    )


def retention_step(
    normed_in, positions, state, query_weight, key_weight, value_weight, head_index, head_total
):
    row_count, head_count, key_size, value_size = state.shape
    query = jnp.dot(normed_in, query_weight, preferred_element_type=jnp.float32).reshape(
        row_count, head_count, key_size
    )
    keys = jnp.dot(normed_in, key_weight, preferred_element_type=jnp.float32).reshape(
        row_count, head_count, key_size
    )
    values = jnp.dot(normed_in, value_weight, preferred_element_type=jnp.float32).reshape(
        row_count, head_count, value_size
    )
    query = rotate_heads(query, positions)
    keys = rotate_heads(keys, positions) * key_size ** (-0.5)
    decay = head_decay(head_index, head_total)
    new_state = state * decay[None, :, None, None] + keys[:, :, :, None] * values[:, :, None, :]
    retained = jnp.einsum("shk,shkv->shv", query, new_state)
    centered = retained - jnp.mean(retained, axis=-1, keepdims=True)
    normed = centered * lax.rsqrt(
        jnp.mean(centered * centered, axis=-1, keepdims=True) + GROUP_EPSILON
    )
    return (normed.astype(jnp.bfloat16).reshape(row_count, head_count * value_size), new_state)


LANES = 128
HALF = LANES // 2
LAST_DIMS = (((1,), (1,)), ((), ()))


def await_bytes(ref, semaphore):
    pltpu.make_async_copy(ref, ref, semaphore).wait()


QUARTERS = 4
CHUNK = 512


def other_index(index, count, step):
    if count & (count - 1):
        return lax.rem(index + step, count)
    result = 0
    for bit in range(count.bit_length() - 1):
        own = lax.rem(lax.div(index, 1 << bit), 2)
        result = result + lax.rem(own + ((step >> bit) & 1), 2) * (1 << bit)
    return result


def tail_kernel(
    ep_count,
    tp_count,
    heads_ref,
    token_ref,
    gain_ref,
    gate_ref,
    route_ref,
    out_weight,
    expert_gate,
    expert_up,
    expert_down,
    dense_gate,
    dense_up,
    dense_down,
    out_ref,
    out_w,
    pair_w,
    down_w,
    dense_gate_w,
    dense_up_w,
    dense_down_w,
    partial_out,
    partials,
    mixed_ref,
    gathered,
    normed_ref,
    dense_part,
    dense_parts,
    hidden_ref,
    outgoing,
    sibling_in,
    chip_out,
    arrived,
    sems,
    out_sems,
    line_sems,
    plane_sems,
    pair_sems,
):
    ep = lax.axis_index("ep")
    tp = lax.axis_index("tp")
    rows, width = token_ref.shape
    token_count = ep_count * rows
    col_width = width // tp_count
    tiles = pair_w.shape[0]
    experts = ep_count // QUARTERS
    places = 2 * tp_count
    chips = experts * places
    expert = lax.div(ep, QUARTERS)
    upper = lax.rem(lax.div(ep, 2), 2)
    side = lax.rem(ep, 2)
    place = tp * 2 + upper
    chip = expert * places + place
    own_row = expert * 2 + upper
    sibling = (ep + 1 - 2 * side, tp)
    head_width = heads_ref.shape[1]
    head_chunk = min(CHUNK, head_width)
    head_chunks = head_width // head_chunk
    own_cols = pl.ds(pl.multiple_of(tp * col_width, LANES), col_width)

    def device(expert_to, place_to):
        return (
            expert_to * QUARTERS + lax.rem(place_to, 2) * 2 + side,
            lax.div(place_to, 2),
        )

    def send(source, target, send_sem, receive_sem, to):
        pltpu.make_async_remote_copy(
            src_ref=source,
            dst_ref=target,
            send_sem=send_sem,
            recv_sem=receive_sem,
            device_id=to,
            device_id_type=MESH,
        ).start()

    part_order = list(range(1, tp_count)) + [0]
    for k in part_order:
        part = lax.rem(tp + k, tp_count)
        for r in range(head_chunks):
            span = pl.ds(r * head_chunk, head_chunk)
            cols = pl.ds(pl.multiple_of(part * col_width, LANES), col_width)
            pltpu.make_async_copy(
                out_weight.at[span, cols],
                out_w.at[k, span, :],
                out_sems.at[k * head_chunks + r],
            ).start()

    barrier = pltpu.get_barrier_semaphore()

    def greet(k, carry):
        other = lax.rem(chip + k, chips)
        pl.semaphore_signal(
            barrier,
            inc=1,
            device_id=device(lax.div(other, places), lax.rem(other, places)),
            device_id_type=MESH,
        )
        return carry

    lax.fori_loop(1, chips, greet, 0)
    pl.semaphore_signal(barrier, inc=1, device_id=sibling, device_id_type=MESH)

    def copy_tile(j):
        cols = pl.ds(j * LANES, LANES)
        pltpu.make_async_copy(
            expert_gate.at[0, :, cols], pair_w.at[j, :, pl.ds(0, LANES)], sems.at[0]
        ).start()
        pltpu.make_async_copy(
            expert_up.at[0, :, cols], pair_w.at[j, :, pl.ds(LANES, LANES)], sems.at[0]
        ).start()

    pltpu.make_async_copy(dense_gate, dense_gate_w, sems.at[2]).start()
    pltpu.make_async_copy(dense_up, dense_up_w, sems.at[3]).start()
    for j in range(tiles):
        copy_tile(j)
    pltpu.make_async_copy(expert_down.at[0], down_w, sems.at[1]).start()
    pltpu.make_async_copy(dense_down, dense_down_w, sems.at[4]).start()

    for k in part_order:
        part = lax.rem(tp + k, tp_count)
        total = jnp.zeros((rows, col_width), jnp.float32)
        for r in range(head_chunks):
            span = pl.ds(r * head_chunk, head_chunk)
            await_bytes(out_w.at[k, span, :], out_sems.at[k * head_chunks + r])
            total = total + jnp.dot(
                heads_ref[:, span], out_w[k, span, :], preferred_element_type=jnp.float32
            )
        if k:
            partial_out[k - 1] = total
            if k == 1:
                pl.semaphore_wait(barrier, chips)
            send(partial_out.at[k - 1], partials.at[tp], sems.at[5], sems.at[6], (ep, part))
        else:
            partials[tp] = total
    await_bytes(partials.at[pl.ds(0, tp_count - 1)], sems.at[6])

    mixed = token_ref[:, own_cols].astype(jnp.float32) + jnp.sum(partials[...], axis=0)
    mixed_ref[...] = mixed
    raised = mixed * gain_ref[:, own_cols]
    squares = jnp.sum(mixed * mixed, axis=-1, keepdims=True)
    along = jnp.sum(raised * gate_ref[:, own_cols], axis=-1, keepdims=True)
    lane = lax.broadcasted_iota(jnp.int32, (rows, LANES), 1)
    factors = jnp.where(lane == HALF - 1, along, route_ref[...])
    factors = jnp.where(lane == HALF - 2, squares, factors)
    high = factors.astype(jnp.bfloat16).astype(jnp.float32)
    low = pltpu.roll(factors - high, HALF, 1)
    gathered[side, expert, place, :, pl.ds(0, col_width)] = raised.astype(jnp.bfloat16)
    gathered[side, expert, place, :, pl.ds(col_width, LANES)] = jnp.where(
        lane < HALF, high, low
    ).astype(jnp.bfloat16)

    own_block = gathered.at[side, expert, place]
    one_block = gathered.at[0, 0, 0]
    others = [other_index(expert, experts, step) for step in range(1, experts)]
    for other in others:
        send(own_block, own_block, sems.at[7], line_sems.at[expert], device(other, place))

    def to_plane(block_expert):
        block = gathered.at[side, block_expert, place]

        def one(k, carry):
            place_to = lax.rem(place + k, places)
            send(
                block, block, sems.at[8], plane_sems.at[block_expert], device(expert, place_to)
            )
            return carry

        lax.fori_loop(1, places, one, 0)

    to_plane(expert)
    for other in others:
        await_bytes(one_block, line_sems.at[other])
        to_plane(other)
    for block_expert in [expert] + others:
        await_bytes(gathered.at[0, 0, pl.ds(0, places - 1)], plane_sems.at[block_expert])
        send(
            gathered.at[side, block_expert],
            gathered.at[side, block_expert],
            sems.at[9],
            sems.at[10],
            sibling,
        )
    await_bytes(gathered.at[0], sems.at[10])

    lane_place = lax.rem(lax.broadcasted_iota(jnp.int32, (token_count, LANES), 1), HALF)
    summed = jnp.zeros((token_count, LANES), jnp.float32)
    for t in range(tp_count):
        pair = pl.ds(2 * t, 2)
        normed_ref[:, pl.ds(t * col_width, col_width)] = (
            gathered[:, :, pair, :, pl.ds(0, col_width)]
            .astype(jnp.float32)
            .reshape(token_count, col_width)
            .astype(jnp.bfloat16)
        )
        tail_lanes = (
            gathered[:, :, pair, :, pl.ds(col_width, LANES)]
            .astype(jnp.float32)
            .reshape(token_count, LANES)
        )
        summed = summed + tail_lanes

    def lanes_sum(values, where):
        return jnp.sum(jnp.where(lane_place == where, values, 0.0), axis=1, keepdims=True)

    expert_factor = lanes_sum(tail_lanes, expert)
    scale = lax.rsqrt(lanes_sum(summed, HALF - 2) / width + RMS_EPSILON)
    branch_factor = 1.0 / (1.0 + jnp.exp(-scale * lanes_sum(summed, HALF - 1)))

    await_bytes(dense_gate_w, sems.at[2])
    await_bytes(dense_up_w, sems.at[3])
    feature_values = normed_ref[:, own_cols]
    for index, weight in ((0, dense_gate_w), (1, dense_up_w)):
        dense_part[index] = (
            scale
            * lax.dot_general(
                feature_values, weight[...], LAST_DIMS, preferred_element_type=jnp.float32
            )
        ).astype(jnp.bfloat16)
    pltpu.make_async_copy(dense_part, dense_parts.at[tp], sems.at[12]).start()

    def share_dense(k, carry):
        send(
            dense_part,
            dense_parts.at[tp],
            sems.at[11],
            sems.at[12],
            (ep, lax.rem(tp + k, tp_count)),
        )
        return carry

    lax.fori_loop(1, tp_count, share_dense, 0)

    await_bytes(pair_w, sems.at[0])

    def expert_tile(j, carry):
        both = scale * jnp.dot(normed_ref[...], pair_w[j], preferred_element_type=jnp.float32)
        gate_value, up_value = both[:, :LANES], both[:, LANES:]
        hidden_ref[:, pl.ds(pl.multiple_of(j * LANES, LANES), LANES)] = (
            gate_value / (1.0 + jnp.exp(-gate_value)) * up_value
        ).astype(jnp.bfloat16)
        return carry

    lax.fori_loop(0, tiles, expert_tile, 0)
    await_bytes(down_w, sems.at[1])
    step = min(2 * LANES, col_width)

    def expert_cols(part, t):
        cols = pl.ds(pl.multiple_of(part * col_width + t * step, LANES), step)
        return expert_factor * jnp.dot(
            hidden_ref[...], down_w[:, cols], preferred_element_type=jnp.float32
        )

    def put(part, t, value):
        outgoing[part, :, :, :, pl.ds(pl.multiple_of(t * step, LANES), step)] = value.reshape(
            2, 2 * experts, rows, step
        ).astype(jnp.bfloat16)

    def to_sibling(part):
        send(
            outgoing.at[part, 1 - side],
            sibling_in.at[part],
            sems.at[13],
            pair_sems.at[part],
            sibling,
        )

    def send_out(part, first):
        await_bytes(sibling_in.at[part], pair_sems.at[part])
        chip_out[part] = (
            outgoing[part, side].astype(jnp.float32) + sibling_in[part].astype(jnp.float32)
        ).astype(jnp.bfloat16)

        def one(k, carry):
            to = lax.rem(own_row + k, 2 * experts)
            send(
                chip_out.at[part, to],
                arrived.at[chip],
                sems.at[14],
                sems.at[15],
                (to * 2 + side, part),
            )
            return carry

        lax.fori_loop(first, 2 * experts, one, 0)

    def other_part(k, carry):
        part = lax.rem(tp + k, tp_count)

        def tile(t, inner):
            put(part, t, expert_cols(part, t))
            return inner

        lax.fori_loop(0, col_width // step, tile, 0)
        to_sibling(part)
        return carry

    lax.fori_loop(1, tp_count, other_part, 0)

    await_bytes(dense_parts, sems.at[12])
    await_bytes(dense_down_w, sems.at[4])
    whole = jnp.sum(dense_parts[...].astype(jnp.float32), axis=0)
    dense_hidden = (whole[0] / (1.0 + jnp.exp(-whole[0])) * whole[1]).astype(jnp.bfloat16)

    def send_other(k, carry):
        send_out(lax.rem(tp + k, tp_count), 0)
        return carry

    lax.fori_loop(1, tp_count, send_other, 0)

    def own_tile(t, carry):
        cols = pl.ds(pl.multiple_of(t * step, LANES), step)
        dense = jnp.dot(dense_hidden, dense_down_w[:, cols], preferred_element_type=jnp.float32)
        put(tp, t, expert_cols(tp, t) + branch_factor * dense)
        return carry

    lax.fori_loop(0, col_width // step, own_tile, 0)
    to_sibling(tp)
    send_out(tp, 1)
    arrived[chip] = chip_out[tp, own_row]
    await_bytes(arrived.at[pl.ds(0, chips - 1)], sems.at[15])

    def gather_sum(i, total):
        return total + jnp.sum(arrived[pl.ds(i * 8, 8)].astype(jnp.float32), axis=0)

    out_ref[...] = lax.fori_loop(0, chips // 8, gather_sum, mixed_ref[...]).astype(out_ref.dtype)
    await_bytes(partials.at[pl.ds(0, tp_count - 1)], sems.at[5])
    if experts > 1:
        await_bytes(gathered.at[0, pl.ds(0, experts - 1), 0], sems.at[7])
    await_bytes(gathered.at[0, :, pl.ds(0, places - 1)], sems.at[8])
    await_bytes(gathered.at[0], sems.at[9])
    await_bytes(dense_parts.at[pl.ds(0, tp_count - 1)], sems.at[11])
    await_bytes(sibling_in, sems.at[13])
    await_bytes(arrived.at[pl.ds(0, chips - 1)], sems.at[14])


def tail(*operands):
    *arrays, ep_count, tp_count = operands
    heads, tokens = arrays[0], arrays[1]
    out_weight = arrays[5]
    expert_gate, expert_down, dense_gate, dense_down = arrays[6], arrays[8], arrays[9], arrays[11]
    rows, width = tokens.shape
    token_count = ep_count * rows
    col_width = width // tp_count
    expert_hidden = expert_gate.shape[2]
    dense_hidden = dense_gate.shape[0]
    experts = ep_count // QUARTERS
    head_width = heads.shape[1]
    head_chunks = head_width // min(CHUNK, head_width)
    bf16, f32 = jnp.bfloat16, jnp.float32
    vmem = pl.BlockSpec(memory_space=pltpu.VMEM)
    in_hbm = pl.BlockSpec(memory_space=pltpu.HBM)
    return pl.pallas_call(
        functools.partial(tail_kernel, ep_count, tp_count),
        out_shape=jax.ShapeDtypeStruct((rows, col_width), bf16),
        in_specs=[vmem] * 5 + [in_hbm] * 7,
        out_specs=vmem,
        scratch_shapes=[
            pltpu.VMEM((tp_count, head_width, col_width), bf16),
            pltpu.VMEM((expert_hidden // LANES, width, 2 * LANES), bf16),
            pltpu.VMEM(expert_down.shape[1:], bf16),
            pltpu.VMEM(dense_gate.shape, bf16),
            pltpu.VMEM(dense_gate.shape, bf16),
            pltpu.VMEM(dense_down.shape, bf16),
            pltpu.VMEM((tp_count - 1, rows, col_width), f32),
            pltpu.VMEM((tp_count, rows, col_width), f32),
            pltpu.VMEM((rows, col_width), f32),
            pltpu.VMEM((2, experts, 2 * tp_count, rows, col_width + LANES), bf16),
            pltpu.VMEM((token_count, width), bf16),
            pltpu.VMEM((2, token_count, dense_hidden), bf16),
            pltpu.VMEM((tp_count, 2, token_count, dense_hidden), bf16),
            pltpu.VMEM((token_count, expert_hidden), bf16),
            pltpu.VMEM((tp_count, 2, 2 * experts, rows, col_width), bf16),
            pltpu.VMEM((tp_count, 2 * experts, rows, col_width), bf16),
            pltpu.VMEM((tp_count, 2 * experts, rows, col_width), bf16),
            pltpu.VMEM((experts * 2 * tp_count, rows, col_width), bf16),
            pltpu.SemaphoreType.DMA((16,)),
            pltpu.SemaphoreType.DMA((tp_count * head_chunks,)),
            pltpu.SemaphoreType.DMA((experts,)),
            pltpu.SemaphoreType.DMA((experts,)),
            pltpu.SemaphoreType.DMA((tp_count,)),
        ],
        compiler_params=pltpu.CompilerParams(
            collective_id=0, has_side_effects=True, vmem_limit_bytes=62 * 1024 * 1024
        ),
    )(*arrays)


def local(
    tokens,
    past_lengths,
    state,
    norm1_gain,
    query_weight,
    key_weight,
    value_weight,
    out_weight,
    norm2_gain,
    branch_gate,
    route_ids,
    route_weights,
    expert_gate,
    expert_up,
    expert_down,
    dense_gate,
    dense_up,
    dense_down,
):
    tp_count = lax.axis_size("tp")
    ep_count = lax.axis_size("ep")
    heads_here = state.shape[1]
    head_index = lax.axis_index("tp") * heads_here + jnp.arange(heads_here)
    inputs = tokens.astype(jnp.float32)
    normed_in = (
        inputs
        * lax.rsqrt(jnp.mean(inputs * inputs, axis=-1, keepdims=True) + RMS_EPSILON)
        * norm1_gain
    ).astype(jnp.bfloat16)
    normed, new_state = retention_step(
        normed_in,
        past_lengths,
        state,
        query_weight,
        key_weight,
        value_weight,
        head_index,
        heads_here * tp_count,
    )
    lanes = jnp.arange(LANES, dtype=jnp.int32)
    named = (route_ids[:, :, None] == lanes[None, None, :]).astype(jnp.float32)
    route_lanes = jnp.sum(named * route_weights[:, :, None], axis=1)
    hidden_pad = -expert_gate.shape[2] % LANES
    if hidden_pad:
        expert_gate = jnp.pad(expert_gate, ((0, 0), (0, 0), (0, hidden_pad)))
        expert_up = jnp.pad(expert_up, ((0, 0), (0, 0), (0, hidden_pad)))
        expert_down = jnp.pad(expert_down, ((0, 0), (0, hidden_pad), (0, 0)))
    layer_out = tail(
        normed,
        tokens,
        norm2_gain[None, :],
        branch_gate[None, :],
        route_lanes,
        out_weight,
        expert_gate,
        expert_up,
        expert_down,
        dense_gate.T,
        dense_up.T,
        dense_down,
        ep_count,
        tp_count,
    )
    return (layer_out, new_state)


def solution(mesh):
    return jax.shard_map(
        local,
        mesh=mesh,
        in_specs=(
            P("ep", None),
            P("ep"),
            P("ep", "tp", None, None),
            P(),
            P(None, "tp"),
            P(None, "tp"),
            P(None, "tp"),
            P("tp", None),
            P(),
            P(),
            P("ep", None),
            P("ep", None),
            P("ep", None, "tp"),
            P("ep", None, "tp"),
            P("ep", "tp", None),
            P("tp", "ep"),
            P("tp", "ep"),
            P("ep", "tp"),
        ),
        out_specs=(P("ep", "tp"), P("ep", "tp", None, None)),
        check_vma=False,
    )
```

time: 66.6 us -> 56.2 us (0.84)
  Pallas kernels: 42.2 us -> 34 us
  matrix products: 10.7 us -> 8.91 us
  local copies, waits for them, and re-layouts: 5.35 us -> 4.25 us
    pallas_call x1, Pallas kernels: 42.2 us -> 34 us  [tail(): pl.pallas_call(functools.partial(tail_kernel, ep_count, tp_count), out_sh...]
    dot_general x1 -> x0, matrix products: 1.81 us -> none  [local(): jnp.dot(normed, out_weight, preferred_element_type=jnp.float32)]
    unnamed x18 -> x13, local copies, waits for them, and re-layouts: 5.31 us -> 4.21 us
    convert_element_type x0 -> x1, other arithmetic: none -> 0.69 us  [retention_step(): normed.astype(jnp.bfloat16).reshape(row_count, head_count * value_size)]
where the time goes in v1:
time: 56.2 us; the launch traced here: 55.8 us
  Pallas kernels  34 us (60%)
  matrix products  8.91 us (16%)
  other arithmetic  7.92 us (14%)
  local copies, waits for them, and re-layouts  4.25 us (8%)
  between operations  0.74 us (1%)
    pallas_call x1, Pallas kernels, tail(): pl.pallas_call(functools.partial(tail_kernel, ep_count, tp_count), out_sh...  34 us
    dot_general x1, matrix products, retention_step(): jnp.dot(normed_in, value_weight, preferred_element_type=jnp.float32)  4.64 us
    add x1, other arithmetic, retention_step(): state * decay[None, :, None, None]  4.27 us
    unnamed x13, local copies, waits for them, and re-layouts  4.21 us
    dot_general x1, matrix products, retention_step(): jnp.dot(normed_in, key_weight, preferred_element_type=jnp.float32)  2.91 us

profile of v1, /device:TPU:0, one launch (start us, length us, event | category | flops | bytes accessed | tf_op | source)
XLA Modules:
  0.0 55.8 jit_solution(14778770791735968215)
XLA Ops:
  0.6 0.9 %fusion = f32[8]{0:T(128)S(1)} fusion(bf16[8,2048]{1,0:T(8,128)(2,1)} %token_ref.1), kind=kLoop, calls=%fused_computation.5 | loop fusion | flops 49144 | bytes 32800 | tf_op jit(solution)/shard_map/reduce_sum | solution.py:503
  1.5 2.9 %convolution_bitcast_fusion = f32[8,8,128]{2,0,1:T(8,128)S(1)} fusion(bf16[2048,1024]{1,0:T(8,128)(2,1)} %param.23, bf16[8,2048]{1,0:T(8,128)(2,1)} %token_ref.1, f32[2048]{0:T(1024)} %param.21, f32[8]{0:T(128)S(1)} %add_rsqrt_fusion.1), kind=kOutput, calls=%fused_computation.1 | convolution fusion | flops 33619968 | bytes 4268064 | tf_op jit(solution)/shard_map/dot_general | solution.py:46
  4.4 0.7 %convert_element_type.23 = f32[8]{0:T(128)S(1)} convert(s32[8]{0:T(128)} %param.19) | non-fusion elementwise | flops 8 | bytes 64 | tf_op jit(solution)/shard_map/convert_element_type | solution.py:25
  5.1 0.1 multiply_cosine_fusion
  5.2 0.1 multiply_subtract_fusion
  5.3 0.1 maximum_multiply_fusion
  5.4 4.6 %fusion.5 = f32[8,2048]{1,0:T(8,128)S(1)} fusion(bf16[2048,2048]{1,0:T(8,128)(2,1)} %param.24, bf16[8,2048]{1,0:T(8,128)(2,1)} %token_ref.1, f32[2048]{0:T(1024)} %param.21, f32[8]{0:T(128)S(1)} %add_rsqrt_fusion.1), kind=kOutput, calls=%fused_computation.29 | convolution fusion | flops 67174400 | bytes 8495136 | tf_op jit(solution)/shard_map/dot_general | solution.py:49
  10.1 0.0 copy-start.1
  10.1 0.0 copy-start.2
  10.1 0.0 copy-start.3
  10.2 4.3 %multiply_add_fusion = f32[8,8,128,256]{3,2,1,0:T(8,128)S(1)} fusion(f32[8,8,128,256]{3,2,1,0:T(8,128)} %param.20, f32[8,8,256]{2,1,0:T(8,128)S(1)} %copy.25, f32[8,8,128]{2,1,0:T(8,128)S(1)} %copy.24, f32[8]{0:T(128)S(1)} %log-plus-one_exponential_fusion), kind=kLoop, calls=%fused_computation | loop fusion | flops 6291456 | bytes 16875552 | tf_op jit(solution)/shard_map/add | solution.py:55
  14.4 0.3 copy-done.1
  14.8 0.0 copy-done.2
  14.8 0.0 copy-done.3
  14.8 0.0 copy-start
  14.8 0.0 copy-start.4
  14.8 0.0 copy-start.5
  14.8 0.7 %convolution_bitcast_fusion.1 = f32[8,8,128]{2,0,1:T(8,128)S(1)} fusion(bf16[2048,1024]{1,0:T(8,128)(2,1)S(1)} %copy-done.1, bf16[8,2048]{1,0:T(8,128)(2,1)S(1)} %copy-done.2, f32[2048]{0:T(1024)S(1)} %copy-done.3, f32[8]{0:T(128)S(1)} %add_rsqrt_fusion.1), kind=kOutput, calls=%fused_computation.2 | convolution fusion | flops 33619968 | bytes 4268064 | tf_op jit(solution)/shard_map/dot_general | solution.py:43
  15.5 0.1 multiply_subtract_fusion.1
  15.6 0.1 maximum_bitcast_fusion
  15.7 2.5 %copy-done = f32[8,8,128,256]{3,2,1,0:T(8,128)} copy-done((f32[8,8,128,256]{3,2,1,0:T(8,128)}, f32[8,8,128,256]{3,2,1,0:T(8,128)S(1)}, u32[]{:S(2)}) %copy-start) | copy-done | bytes 8388632
  18.2 0.7 %fusion.3 = f32[8,8,1,256]{3,2,1,0:T(1,128)S(1)} fusion(f32[8,8,128,256]{3,2,1,0:T(8,128)S(1)} %multiply_add_fusion, bf16[8,8,128,1]{2,0,1,3:T(8,128)(2,1)S(1)} %maximum_bitcast_fusion), kind=kOutput, calls=%fused_computation.14 | convolution fusion | flops 4194304 | bytes 8470528 | tf_op jit(solution)/shard_map/shk,shkv->shv/dot_general | solution.py:56
  18.8 0.1 bitcast_reduce_fusion
  19.0 0.2 multiply_reduce_fusion
  19.1 0.7 %multiply_convert_fusion = bf16[8,8,256]{2,0,1:T(8,128)(2,1)} fusion(f32[8,8,1,256]{3,2,1,0:T(1,128)S(1)} %fusion.3, f32[8,8]{0,1:T(8,128)S(1)} %add_rsqrt_fusion, f32[8,8]{0,1:T(8,128)S(1)} %broadcast_multiply_fusion), kind=kLoop, calls=%fused_computation.10 | loop fusion | flops 49152 | bytes 98816 | tf_op jit(solution)/shard_map/convert_element_type | solution.py:61
  19.8 0.0 copy-done.4
  19.8 0.0 copy-done.5
  19.8 0.7 %select_reduce_fusion.route_ref = f32[8,128]{1,0:T(8,128)} fusion(f32[8,2]{0,1:T(2,128)S(1)} %copy-done.4, s32[8,2]{0,1:T(2,128)S(1)} %copy-done.5), kind=kLoop, calls=%fused_computation.20 | loop fusion | flops 5120 | bytes 4224 | tf_op jit(solution)/shard_map/reduce_sum | solution.py:518
  20.5 34.0 %shard_map.185 = bf16[8,1024]{1,0:T(8,128)(2,1)} custom-call(bf16[8,2048]{1,0:T(8,128)(2,1)} %bitcast.26, bf16[8,2048]{1,0:T(8,128)(2,1)} %token_ref.1, f32[1,2048]{1,0:T(1,128)} %bitcast.27, f32[1,2048]{1,0:T(1,128)} %bitcast.28, f32[8,128]{1,0:T(8,128)} %select_reduce_fusion.route_ref, bf16[2048,2048]{1,0:T(8,128)(2,1)} %out_weight.1, ...), custom_call_target="tpu_custom_call" | custom-call | tf_op jit(solution)/shard_map/pallas_call | solution.py:440
  54.5 1.3 %copy.34 = bf16[8,1024]{1,0:T(8,128)(2,1)} copy(bf16[8,1024]{1,0:T(8,128)(2,1)} %shard_map.185) | data formatting | bytes 32768
  (7 shorter events, 0.1 us)
Async XLA Ops:
  10.1 4.7 %copy-start.1 = (bf16[2048,1024]{1,0:T(8,128)(2,1)S(1)}, bf16[2048,1024]{1,0:T(8,128)(2,1)}, u32[]{:S(2)}) copy-start(bf16[2048,1024]{1,0:T(8,128)(2,1)} %param.22) | copy-start | bytes 12582916
  10.1 4.6 %copy-start.2 = (bf16[8,2048]{1,0:T(8,128)(2,1)S(1)}, bf16[8,2048]{1,0:T(8,128)(2,1)}, u32[]{:S(2)}) copy-start(bf16[8,2048]{1,0:T(8,128)(2,1)} %token_ref.1) | copy-start | bytes 98308
  10.1 4.6 %copy-start.3 = (f32[2048]{0:T(1024)S(1)}, f32[2048]{0:T(1024)}, u32[]{:S(2)}) copy-start(f32[2048]{0:T(1024)} %param.21) | copy-start | bytes 24580
  14.8 3.4 %copy-start = (f32[8,8,128,256]{3,2,1,0:T(8,128)}, f32[8,8,128,256]{3,2,1,0:T(8,128)S(1)}, u32[]{:S(2)}) copy-start(f32[8,8,128,256]{3,2,1,0:T(8,128)S(1)} %multiply_add_fusion) | copy-start | bytes 25165828
  14.8 5.0 %copy-start.4 = (f32[8,2]{0,1:T(2,128)S(1)}, f32[8,2]{0,1:T(2,128)}, u32[]{:S(2)}) copy-start(f32[8,2]{0,1:T(2,128)} %param.29) | copy-start | bytes 196
  14.8 5.0 %copy-start.5 = (s32[8,2]{0,1:T(2,128)S(1)}, s32[8,2]{0,1:T(2,128)}, u32[]{:S(2)}) copy-start(s32[8,2]{0,1:T(2,128)} %param.28) | copy-start | bytes 196
